TPU v7x, 32 devices: a whole 2x2x4 slice. The times are simulated.
32 devices in a mesh: sp: 4 (over y, x), tp: 8 (over z, core).
Axes of the slice: x: 2, y: 2, z: 4, core: 2. Of those that a mesh axis runs over, the one named last changes fastest.
Arguments:
- queries: bfloat16 [1536, 2048], P('sp', 'tp'), may hold values from -6 to 6
- keys: bfloat16 [1536, 2048], P('sp', 'tp'), may hold values from -6 to 6
- values: bfloat16 [1536, 2048], P('sp', 'tp'), may hold values from -6 to 6
- key_bias: bfloat16 [1536, 32], P('sp', 'tp'), may hold values from -16 to 0
- head_gain: float32 [32, 64], P('tp'), may hold values from 0.1 to 1.9
- out_weight: bfloat16 [2048, 2048], P('tp'), may hold values from -0.125 to 0.125
- residual: bfloat16 [1536, 2048], P(('sp', 'tp')), may hold values from -6 to 6
- norm_gain: float32 [2048], replicated, may hold values from 0.1 to 1.9
- gate_proj: bfloat16 [4, 2048, 7168], P('sp', None, 'tp'), may hold values from -0.125 to 0.125
- up_proj: bfloat16 [4, 2048, 7168], P('sp', None, 'tp'), may hold values from -0.125 to 0.125
- down_proj: bfloat16 [4, 7168, 2048], P('sp', 'tp'), may hold values from -0.0625 to 0.0625
- expert_choice: int32 [1536, 2], P(('sp', 'tp')), may hold values from 0 to 3, all different within a row; in each aligned block of 48 rows (0 to 47, 48 to 95, ...) at most 48 rows name the same one
- expert_weights: float32 [1536, 2], P(('sp', 'tp')), may hold values from 0.2 to 1
Outputs:
- layer_out: bfloat16 [1536, 2048], P(('sp', 'tp'))
Inputs may be any that keep to these rules, and one draw needn't show every extreme that they name: `expert_choice`: in each aligned block of 48 rows (the rows of one device), no expert is named more than 48 times; the two experts of a row differ.
All inputs are finite; a program needn't handle non-finite values.
Results may differ from a plain program's by a relative error of at most 0.019.
Values may be sent and summed in bfloat16 or wider, within the bound.
A program may use at most 128 MiB of HBM per device.

v0:
```python
import jax
import jax.numpy as jnp
from jax import lax
from jax.sharding import PartitionSpec as P

epsilon = 1e-06


def rms_scaled(values_in):
    return values_in * lax.rsqrt(jnp.mean(values_in * values_in, axis=-1, keepdims=True) + epsilon)


def expert_partial(row_block, gate_matrix, up_matrix, down_matrix):
    gate_part = jnp.dot(row_block, gate_matrix, preferred_element_type=jnp.float32)
    up_part = jnp.dot(row_block, up_matrix, preferred_element_type=jnp.float32)
    hidden = (jax.nn.silu(gate_part) * up_part).astype(jnp.bfloat16)
    return jnp.dot(hidden, down_matrix, preferred_element_type=jnp.float32)


def choice_ranks(routes, experts_all):
    flat_routes = routes.reshape(routes.shape[:-2] + (-1,))
    onehot = (flat_routes[..., None] == jnp.arange(experts_all, dtype=jnp.int32)).astype(jnp.int32)
    before = jnp.cumsum(onehot, axis=-2) - onehot
    return jnp.sum(before * onehot, axis=-1).reshape(routes.shape)


def slot_tokens(slot_index, targets, missing):
    flat_slots = slot_index.reshape(-1)
    owners = jnp.arange(flat_slots.shape[0], dtype=jnp.int32) // 2
    matches = flat_slots[None, :] == jnp.arange(targets, dtype=jnp.int32)[:, None]
    owner_found = jnp.sum(jnp.where(matches, owners[None, :], 0), axis=1)
    return jnp.where(jnp.any(matches, axis=1), owner_found, missing)


def on_device(
    queries,
    keys,
    values,
    key_bias,
    head_gain,
    out_weight,
    residual,
    norm_gain,
    gate_proj,
    up_proj,
    down_proj,
    expert_choice,
    expert_weights,
):
    rows_own = queries.shape[0]
    heads_here = head_gain.shape[0]
    head_size = head_gain.shape[1]
    model_width = out_weight.shape[1]
    seq_devices = lax.axis_size("sp")
    head_devices = lax.axis_size("tp")
    own_start = lax.axis_index("sp") * rows_own
    query_pos = own_start + jnp.arange(rows_own, dtype=jnp.int32)
    query_heads = queries.reshape(rows_own, heads_here, head_size)

    def key_block(slot_state, key_rows, value_rows, bias_rows, key_start):
        key_heads = key_rows.reshape(rows_own, heads_here, head_size)
        value_heads = value_rows.reshape(rows_own, heads_here, head_size)
        scores = jnp.einsum(
            "qhd,khd->hqk", query_heads, key_heads, preferred_element_type=jnp.float32
        ) * head_size ** (-0.5)
        scores = scores + bias_rows.astype(jnp.float32).T[:, None, :]
        key_pos = key_start + jnp.arange(rows_own, dtype=jnp.int32)
        earlier = (key_pos[None, :] < query_pos[:, None])[None, :, :]
        log_drops = jnp.where(earlier, jax.nn.log_sigmoid(-scores), 0.0)
        suffix = lax.cumsum(log_drops, axis=2, reverse=True) - log_drops
        within = jnp.where(earlier, jnp.exp(jax.nn.log_sigmoid(scores) + suffix), 0.0).astype(
            jnp.bfloat16
        )
        block_part = jnp.einsum(
            "hqk,khd->qhd", within, value_heads, preferred_element_type=jnp.float32
        )
        block_index = key_start // rows_own
        sums_new = lax.dynamic_update_index_in_dim(
            slot_state[0], block_part.reshape(rows_own, heads_here * head_size), block_index, 0
        )
        totals_new = lax.dynamic_update_index_in_dim(
            slot_state[1], jnp.sum(log_drops, axis=2), block_index, 0
        )
        return (sums_new, totals_new)

    empty_state = (
        jnp.zeros((seq_devices, rows_own, heads_here * head_size), jnp.float32),
        jnp.zeros((seq_devices, heads_here, rows_own), jnp.float32),
    )
    key_piece = lax.all_gather(keys, "sp", axis=0, tiled=True)
    value_piece = lax.all_gather(values, "sp", axis=0, tiled=True)
    bias_piece = lax.all_gather(key_bias, "sp", axis=0, tiled=True)

    def visit(block_count, state_in):
        offset = block_count * rows_own

        def take_rows(array):
            return lax.dynamic_slice_in_dim(array, offset, rows_own, 0)

        def compute(state_now):
            return key_block(
                state_now,
                take_rows(key_piece),
                take_rows(value_piece),
                take_rows(bias_piece),
                offset,
            )

        def keep(state_now):
            return state_now

        return lax.cond(offset <= own_start, compute, keep, state_in)

    block_sums, totals = lax.fori_loop(0, key_piece.shape[0] // rows_own, visit, empty_state)
    carried = jnp.sum(totals, axis=0, keepdims=True) - jnp.cumsum(totals, axis=0)
    factors = jnp.exp(carried).transpose(0, 2, 1)[..., None]
    mixture = jnp.sum(
        factors * block_sums.reshape(seq_devices, rows_own, heads_here, head_size), axis=0
    )
    attended = (
        (rms_scaled(mixture) * head_gain)
        .astype(jnp.bfloat16)
        .reshape(rows_own, heads_here * head_size)
    )
    row_share = rows_own // head_devices
    merged = lax.all_to_all(attended, "tp", split_axis=0, concat_axis=1, tiled=True)
    projected = jnp.dot(
        merged,
        lax.all_gather(out_weight, "tp", axis=0, tiled=True),
        preferred_element_type=jnp.float32,
    )
    stream = (residual.astype(jnp.float32) + projected).astype(jnp.bfloat16)
    normed = (rms_scaled(stream.astype(jnp.float32)) * norm_gain).astype(jnp.bfloat16)
    local_experts = gate_proj.shape[0]
    experts_all = local_experts * seq_devices
    capacity = 4 * rows_own // (head_devices * experts_all)
    own_slots = expert_choice * capacity + choice_ranks(expert_choice, experts_all)
    wanted = slot_tokens(own_slots, experts_all * capacity, row_share)
    outgoing = jnp.take(normed, wanted, axis=0, mode="fill", fill_value=0)
    arrived = lax.all_to_all(
        outgoing.reshape(seq_devices, local_experts, capacity, model_width),
        "sp",
        split_axis=0,
        concat_axis=0,
        tiled=True,
    )
    row_piece = lax.all_gather(arrived, "tp", axis=0, tiled=True)
    count_rows = row_piece.shape[0]
    partials = jnp.stack(
        [
            expert_partial(
                row_piece[:, 0].reshape(-1, model_width), gate_proj[0], up_proj[0], down_proj[0]
            ).reshape(count_rows, capacity, model_width)
        ],
        axis=1,
    )
    summed = lax.psum_scatter(partials.astype(jnp.bfloat16), "tp", scatter_dimension=0, tiled=True)
    returned = lax.all_to_all(summed, "sp", split_axis=0, concat_axis=0, tiled=True).reshape(
        experts_all * capacity, model_width
    )
    picked = jnp.take(returned, own_slots, axis=0).astype(jnp.float32)
    combined = jnp.sum(expert_weights[:, :, None] * picked, axis=1)
    return (stream.astype(jnp.float32) + combined).astype(jnp.bfloat16)


def solution(mesh):
    placed = (
        P("sp", "tp"),
        P("sp", "tp"),
        P("sp", "tp"),
        P("sp", "tp"),
        P("tp", None),
        P("tp", None),
        P(("sp", "tp"), None),
        P(),
        P("sp", None, "tp"),
        P("sp", None, "tp"),
        P("sp", "tp", None),
        P(("sp", "tp"), None),
        P(("sp", "tp"), None),
    )
    return jax.shard_map(
        on_device, mesh=mesh, in_specs=placed, out_specs=P(("sp", "tp"), None), check_vma=False
    )
```

profile of v0, /device:TPU:0, one launch (start us, length us, event | category | flops | bytes accessed | tf_op | source)
XLA Modules:
  0.0 380.5 jit_solution(13210839301603181166)
XLA Ops:
  6.5 0.7 all-gather.3.cloned.1.call-update
  7.3 1.1 copy.81
  8.4 1.1 copy.82
  9.4 1.7 copy.83
  11.2 11.0 %all_gather.17 = bf16[1536,4]{0,1:T(4,128)(2,1)} all-gather(bf16[384,4]{0,1:T(4,128)(2,1)} %param.20), channel_id=1, replica_groups=mesh['sp'=4,'tp'=8] {'sp'}, dimensions={0}, use_global_device_ids=true | all-gather | bytes 15360 | tf_op jit(solution)/shard_map/all_gather | solution.py:92
  22.2 12.4 %all_gather.15 = bf16[1536,256]{0,1:T(8,128)(2,1)} all-gather(bf16[384,256]{0,1:T(8,128)(2,1)S(1)} %copy.81), channel_id=1, replica_groups=mesh['sp'=4,'tp'=8] {'sp'}, dimensions={0}, use_global_device_ids=true | all-gather | bytes 983040 | tf_op jit(solution)/shard_map/all_gather | solution.py:91
  34.5 13.4 %all_gather.16 = bf16[1536,256]{0,1:T(8,128)(2,1)} all-gather(bf16[384,256]{0,1:T(8,128)(2,1)S(1)} %copy.82), channel_id=1, replica_groups=mesh['sp'=4,'tp'=8] {'sp'}, dimensions={0}, use_global_device_ids=true | all-gather | bytes 983040 | tf_op jit(solution)/shard_map/all_gather | solution.py:90
  47.9 1.3 broadcast_in_dim.84
  49.2 0.6 broadcast_in_dim.85
  49.8 28.2 %while.17 = (s32[]{:T(128)}, f32[4,384,256]{1,2,0:T(8,128)}, f32[4,4,384]{2,1,0:T(4,128)}, s32[]{:T(128)}, bf16[1536,256]{0,1:T(8,128)(2,1)}, /*index=5*/bf16[15...) while((s32[]{:T(128)}, f32[4,384,256]{1,2,0:T(8,128)}, ...), condition=%wide.region_6.7_spmd.clone.clone, body=%wide.region_0.6_spmd.clone.clone.sunk | while | flops 246117120 | bytes 38572464 | solution.py:114
  49.8 28.0 %conditional.4 = ((f32[4,384,256]{1,2,0:T(8,128)}, f32[4,4,384]{2,1,0:T(4,128)})) conditional(s32[]{:T(128)} %convert_element_type.76, (f32[4,384,256]{1,2,0:T(8,128)}, f32[4,4,384]{2,1,0:T(4,128)}) %tuple.53, (s32[]{:T(128)}, bf16[1536,256]{0,1:T(8,128)(2,1)}, s32[]{:T(128)}, bf16[1536,256]{0,1:T(8,128)(2,1)}, bf16[384,4,64]{0,2,1:T(8,128)(2,1)}, ...), branch_computations={%region_1.0_spmd, %region_2.5_spmd} | conditional | flops 246117120 | bytes 38570716 | solution.py:112
  49.8 1.1 constant_dynamic-slice_fusion
  50.8 0.7 convert_bitcast_fusion
  51.5 0.1 broadcast_compare_fusion
  51.7 4.3 %fusion.15 = (f32[4,384]{1,0:T(4,128)S(1)}, f32[4,384,384]{1,2,0:T(8,128)S(1)}, f32[4,384,384]{2,1,0:T(8,128)}) fusion(f32[4,384]{1,0:T(4,128)S(1)} %convert_bitcast_fusion, pred[384,384]{0,1:T(8,128)(4,1)S(1)} %broadcast_compare_fusion, bf16[384,4,64]{0,2,1:T(8,128)(2,1)S(1)} %bitcast.92, bf16[384,4,64]{0,2,1:T(8,128)(2,1)} %get-tuple-element.177), kind=kOutput, calls=%fused_computation.33 | convolution fusion | flops 81984000 | bytes 5271552 | tf_op jit(solution)/shard_map/while/body/eval_jaxpr/cond/branch_1_fun/qhd,khd->hqk/dot_general | solution.py:63
  56.0 14.0 %fusion.2 = f32[4,384,3,128]{1,2,3,0:T(4,128)S(1)} fusion(f32[4,384,3,128]{1,3,2,0:T(8,128)S(1)} %bitcast.88), kind=kOutput, calls=%fused_computation.5 | output fusion | flops 74907648 | bytes 4718592 | tf_op jit(solution)/shard_map/reduce-window
  70.1 0.5 broadcast_add_fusion
  70.6 0.2 copy.79
  70.9 1.5 copy-done
  72.3 3.6 fusion.8
  76.0 0.3 fusion.27
  76.3 0.8 constant_dynamic-update-slice_fusion
  77.1 0.6 bitcast_dynamic-update-slice_fusion
  78.0 0.8 reduce_sum.74
  78.7 0.8 fusion.24
  79.5 1.6 fusion.22
  81.1 0.2 copy.84
  81.3 0.1 copy.85
  81.5 0.5 mul.104
  81.9 0.5 mul.105
  82.5 0.7 multiply_convert_fusion.2
  83.2 4.8 %all-to-all-start = ((bf16[8,48,256]{2,1,0:T(8,128)(2,1)}), bf16[8,48,256]{2,1,0:T(8,128)(2,1)S(1)}, u32[]{:S(2)}, u32[]{:S(2)}) async-start(bf16[8,48,256]{2,1,0:T(8,128)(2,1)} %multiply_convert_fusion.2), calls=%async_computation | async-start | bytes 393216 | tf_op jit(solution)/shard_map/all_to_all | solution.py:126
  88.5 0.2 select_reduce_fusion.1
  89.5 6.8 %all-to-all-done = bf16[8,48,256]{2,1,0:T(8,128)(2,1)S(1)} async-done(((bf16[8,48,256]{2,1,0:T(8,128)(2,1)}), bf16[8,48,256]{2,1,0:T(8,128)(2,1)S(1)}, u32[]{:S(2)}, u32[]{:S(2)}) %all-to-all-start) | async-done | bytes 196640 | tf_op jit(solution)/shard_map/all_to_all | solution.py:126
  96.4 5.1 %multiply_reduce_fusion.1 = (f32[48]{0:T(128)S(1)}, f32[48,2048]{1,0:T(8,128)S(1)}) fusion(bf16[48,2048]{1,0:T(8,128)(2,1)S(1)} %bitcast.94, bf16[2048,2048]{1,0:T(8,128)(2,1)} %all-gather.3.cloned.1.call-done, bf16[48,2048]{1,0:T(8,128)(2,1)S(1)} %copy-done.1), kind=kOutput, calls=%fused_computation.54 | convolution fusion | flops 403242944 | bytes 9175232 | tf_op jit(solution)/shard_map/dot_general | solution.py:127
  101.6 1.1 gather_fusion
  102.9 96.4 %all_to_all.26 = bf16[4,1,48,2048]{3,2,1,0:T(8,128)(2,1)} all-to-all(bf16[4,1,48,2048]{3,2,1,0:T(8,128)(2,1)S(1)} %broadcast_select_fusion), channel_id=1, replica_groups=mesh['sp'=4,'tp'=8] {'sp'}, dimensions={0} | all-to-all | bytes 1572864 | tf_op jit(solution)/shard_map/all_to_all | solution.py:140
  199.4 63.5 %all-gather.5.cloned.1.call-done = bf16[32,1,48,2048]{3,2,1,0:T(8,128)(2,1)} async-done(((bf16[4,1,48,2048]{3,2,1,0:T(8,128)(2,1)}), bf16[32,1,48,2048]{3,2,1,0:T(8,128)(2,1)}) %all-gather.5.cloned.1.call-update) | async-done | bytes 6291472 | tf_op jit(solution)/shard_map/all_gather | solution.py:147
  262.9 10.0 %fusion.18 = f32[1536,896]{1,0:T(8,128)S(1)} fusion(bf16[1536,2048]{1,0:T(8,128)(2,1)} %bitcast.101, bf16[1,2048,896]{2,1,0:T(8,128)(2,1)} %param.25), kind=kOutput, calls=%fused_computation.38 | convolution fusion | flops 5637144576 | bytes 15466496 | tf_op jit(solution)/shard_map/dot_general | solution.py:14
  272.9 7.1 %multiply_convert_fusion = bf16[1536,896]{1,0:T(8,128)(2,1)S(1)} fusion(f32[1536,896]{1,0:T(8,128)S(1)} %fusion.18, bf16[1536,2048]{1,0:T(8,128)(2,1)S(1)} %bitcast.102, bf16[1,2048,896]{2,1,0:T(8,128)(2,1)S(1)} %copy-done.7), kind=kOutput, calls=%fused_computation.35 | convolution fusion | flops 5645402112 | bytes 18219008 | tf_op jit(solution)/shard_map/dot_general | solution.py:15
  280.0 8.7 %convert_bitcast_fusion.1 = bf16[32,1,48,2048]{3,2,0,1:T(8,128)(2,1)} fusion(bf16[32,48,896]{2,1,0:T(8,128)(2,1)S(1)} %bitcast.103, bf16[1,896,2048]{2,1,0:T(8,128)(2,1)S(1)} %copy-done.8), kind=kOutput, calls=%fused_computation.34 | convolution fusion | flops 5640290304 | bytes 12713984 | tf_op jit(solution)/shard_map/dot_general | solution.py:17
  288.8 68.5 %reduce-scatter.2.cloned.1.call-done = bf16[4,1,48,2048]{3,2,0,1:T(8,128)(2,1)} async-done(((bf16[32,1,48,2048]{3,2,0,1:T(8,128)(2,1)}), bf16[4,1,48,2048]{3,2,0,1:T(8,128)(2,1)}) %reduce-scatter.2.cloned.1.call-update) | async-done | bytes 786448 | tf_op jit(solution)/shard_map/reduce_scatter | solution.py:157
  357.3 3.7 all-to-all-start.2
  361.5 8.6 %all-to-all-done.2 = bf16[4,1,48,2048]{3,2,1,0:T(8,128)(2,1)S(1)} async-done(((bf16[4,1,48,2048]{3,2,1,0:T(8,128)(2,1)}), bf16[4,1,48,2048]{3,2,1,0:T(8,128)(2,1)S(1)}, u32[]{:S(2)}, u32[]{:S(2)}) %all-to-all-start.2) | async-done | bytes 786464 | tf_op jit(solution)/shard_map/all_to_all | solution.py:158
  370.1 0.8 gather_fusion.1
  370.9 0.3 reshape.183
  371.2 2.1 multiply_reduce_fusion
  373.3 0.7 add_convert_fusion
  (64 shorter events, 2.3 us)
Async XLA Ops:
  6.5 89.9 %all-gather.3.cloned.1.call-start = ((), (), s32[]{:S(2)}) async-start(), calls=%async_computation.4 | async-start | bytes 9437184 | tf_op jit(solution)/shard_map/all_gather | solution.py:129
  70.6 1.7 copy-start
  79.5 2.9 copy-start.4
  81.1 7.0 %copy-start.3 = (s32[48,2]{0,1:T(2,128)S(1)}, s32[48,2]{0,1:T(2,128)}, u32[]{:S(2)}) copy-start(s32[48,2]{0,1:T(2,128)} %param.28) | copy-start | bytes 1156
  81.3 15.1 %copy-start.1 = (bf16[48,2048]{1,0:T(8,128)(2,1)S(1)}, bf16[48,2048]{1,0:T(8,128)(2,1)}, u32[]{:S(2)}) copy-start(bf16[48,2048]{1,0:T(8,128)(2,1)} %param.23) | copy-start | bytes 589828
  83.2 13.1 %all-to-all-start = ((bf16[8,48,256]{2,1,0:T(8,128)(2,1)}), bf16[8,48,256]{2,1,0:T(8,128)(2,1)S(1)}, u32[]{:S(2)}, u32[]{:S(2)}) async-start(bf16[8,48,256]{2,1,0:T(8,128)(2,1)} %multiply_convert_fusion.2), calls=%async_computation | async-start | bytes 393216 | tf_op jit(solution)/shard_map/all_to_all | solution.py:126
  88.0 174.9 %all-gather.5.cloned.1.call-start = ((), (), s32[]{:S(2)}) async-start(), calls=%async_computation.5 | async-start | bytes 7077888 | tf_op jit(solution)/shard_map/all_gather | solution.py:147
  96.4 5.1 %copy-start.2 = (f32[2048]{0:T(1024)S(1)}, f32[2048]{0:T(1024)}, u32[]{:S(2)}) copy-start(f32[2048]{0:T(1024)} %param.24) | copy-start | bytes 24580
  199.3 158.0 %reduce-scatter.2.cloned.1.call-start = ((), (), s32[]{:S(2)}) async-start(), calls=%async_computation.6 | async-start | bytes 7077888 | tf_op jit(solution)/shard_map/reduce_scatter | solution.py:157
  262.9 10.0 %copy-start.6 = (bf16[32,1,48,2048]{3,2,1,0:T(8,128)(2,1)S(1)}, bf16[32,1,48,2048]{3,2,1,0:T(8,128)(2,1)}, u32[]{:S(2)}) copy-start(bf16[32,1,48,2048]{3,2,1,0:T(8,128)(2,1)} %all-gather.5.cloned.1.call-done) | copy-start | bytes 18874372
  262.9 10.0 %copy-start.7 = (bf16[1,2048,896]{2,1,0:T(8,128)(2,1)S(1)}, bf16[1,2048,896]{2,1,0:T(8,128)(2,1)}, u32[]{:S(2)}) copy-start(bf16[1,2048,896]{2,1,0:T(8,128)(2,1)} %param.26) | copy-start | bytes 11010052
  272.9 7.1 %copy-start.8 = (bf16[1,896,2048]{2,1,0:T(8,128)(2,1)S(1)}, bf16[1,896,2048]{2,1,0:T(8,128)(2,1)}, u32[]{:S(2)}) copy-start(bf16[1,896,2048]{2,1,0:T(8,128)(2,1)} %param.27) | copy-start | bytes 11010052
  288.8 72.6 %copy-start.5 = (f32[48,2]{0,1:T(2,128)S(1)}, f32[48,2]{0,1:T(2,128)}, u32[]{:S(2)}) copy-start(f32[48,2]{0,1:T(2,128)} %param.29) | copy-start | bytes 1156
  357.3 12.7 %all-to-all-start.2 = ((bf16[4,1,48,2048]{3,2,1,0:T(8,128)(2,1)}), bf16[4,1,48,2048]{3,2,1,0:T(8,128)(2,1)S(1)}, u32[]{:S(2)}, u32[]{:S(2)}) async-start(bf16[4,1,48,2048]{3,2,1,0:T(8,128)(2,1)} %bitcast.96), calls=%async_computation.3 | async-start | bytes 1572864 | tf_op jit(solution)/shard_map/all_to_all | solution.py:158
Sparse Core Ops, SparseCore 0:
  8.9 84.8 all-gather.2
  199.4 63.4 all-gather.4
  288.9 68.3 reduce-scatter.1
where the time goes:
time: 382 us; the launch traced here: 380 us
  waiting for transfers between devices  148 us (39%)
  blocking collectives  133 us (35%)
  matrix products  35.5 us (9%)
  other arithmetic  26.7 us (7%)
  local copies, waits for them, and re-layouts  14.7 us (4%)
  between operations  13.4 us (4%)
  starting transfers between devices  8.62 us (2%)
    all_to_all x1, blocking collectives, on_device(): lax.all_to_all(outgoing.reshape(seq_devices, local_experts, capacity, mod...  96.4 us
    reduce_scatter x1, waiting for transfers between devices, on_device(): lax.psum_scatter(partials.astype(jnp.bfloat16), 'tp', scatter_dimension=0...  68.5 us
    all_gather x1, waiting for transfers between devices, on_device(): row_piece = lax.all_gather(arrived, 'tp', axis=0, tiled=True)  63.5 us
    another operation x2, other arithmetic  14.1 us
    all_gather x1, blocking collectives, on_device(): key_piece = lax.all_gather(keys, 'sp', axis=0, tiled=True)  13.4 us
    all_gather x1, blocking collectives, on_device(): value_piece = lax.all_gather(values, 'sp', axis=0, tiled=True)  12.4 us
    all_gather x1, blocking collectives, on_device(): bias_piece = lax.all_gather(key_bias, 'sp', axis=0, tiled=True)  11 us
    dot_general x1, matrix products, expert_partial(): jnp.dot(row_block, gate_matrix, preferred_element_type=jnp.float32)  9.96 us
  transfers between devices with their start and end apart: 5, of which 4 were waited for; matrix products, arithmetic and copies ran while one was open for 10% of the time, Pallas kernels for 0%

commit v1 on v0

v1 whole, which is shorter than its diff:
```python
import functools

import jax
import jax.numpy as jnp
from jax import lax
from jax.experimental import pallas as pl
from jax.experimental.pallas import tpu as pltpu
from jax.sharding import PartitionSpec as P

epsilon = 1e-06


def rms_scaled(values_in):
    return values_in * lax.rsqrt(jnp.mean(values_in * values_in, axis=-1, keepdims=True) + epsilon)


def expert_partial(row_block, gate_matrix, up_matrix, down_matrix):
    gate_part = jnp.dot(row_block, gate_matrix, preferred_element_type=jnp.float32)
    up_part = jnp.dot(row_block, up_matrix, preferred_element_type=jnp.float32)
    hidden = (jax.nn.silu(gate_part) * up_part).astype(jnp.bfloat16)
    return jnp.dot(hidden, down_matrix, preferred_element_type=jnp.float32)


def choice_ranks(routes, experts_all):
    flat_routes = routes.reshape(routes.shape[:-2] + (-1,))
    onehot = (flat_routes[..., None] == jnp.arange(experts_all, dtype=jnp.int32)).astype(jnp.int32)
    before = jnp.cumsum(onehot, axis=-2) - onehot
    return jnp.sum(before * onehot, axis=-1).reshape(routes.shape)


def slot_tokens(slot_index, targets, missing):
    flat_slots = slot_index.reshape(-1)
    owners = jnp.arange(flat_slots.shape[0], dtype=jnp.int32) // 2
    matches = flat_slots[None, :] == jnp.arange(targets, dtype=jnp.int32)[:, None]
    owner_found = jnp.sum(jnp.where(matches, owners[None, :], 0), axis=1)
    return jnp.where(jnp.any(matches, axis=1), owner_found, missing)


def softplus_parts(scores):
    drops = -jnp.maximum(scores, 0.0) - jnp.log(1.0 + jnp.exp(-jnp.abs(scores)))
    return drops, scores + drops


def attend_block(query_ref, key_of, value_of, bias_of, mix_ref, carry_ref, head_size, diagonal):
    rows, width = query_ref.shape
    lanes = 128 if width % 128 == 0 else width
    per_group = lanes // head_size
    chunk = 128 if rows % 128 == 0 else rows
    later_row = lax.broadcasted_iota(jnp.int32, (rows, rows), 0)
    later_col = lax.broadcasted_iota(jnp.int32, (rows, rows), 1)
    suffix_of = jnp.where(later_row > later_col, 1.0, 0.0).astype(jnp.bfloat16)
    lane_head = lax.broadcasted_iota(jnp.int32, (1, lanes), 1) // head_size
    for group in range(width // lanes):
        cols = slice(group * lanes, (group + 1) * lanes)
        key_tile = key_of(cols)
        value_tile = value_of(cols)
        for inner in range(per_group):
            mine = lane_head == inner
            bias_row = bias_of(group * per_group + inner)
            for start in range(0, rows, chunk):
                span = slice(start, start + chunk)
                query = query_ref[span, cols] * jnp.asarray(head_size**-0.5, jnp.bfloat16)
                query = jnp.where(mine, query, jnp.zeros_like(query))
                scores = lax.dot_general(
                    query, key_tile, (((1,), (1,)), ((), ())), preferred_element_type=jnp.float32
                )
                scores = scores + bias_row
                drops, hits = softplus_parts(scores)
                if diagonal:
                    row_pos = start + lax.broadcasted_iota(jnp.int32, (chunk, rows), 0)
                    col_pos = lax.broadcasted_iota(jnp.int32, (chunk, rows), 1)
                    earlier = col_pos < row_pos
                    drops = jnp.where(earlier, drops, 0.0)
                high = drops.astype(jnp.bfloat16)
                low = (drops - high.astype(jnp.float32)).astype(jnp.bfloat16)
                suffix = jnp.dot(high, suffix_of, preferred_element_type=jnp.float32)
                suffix = suffix + jnp.dot(low, suffix_of, preferred_element_type=jnp.float32)
                within = jnp.exp(hits + suffix)
                if diagonal:
                    within = jnp.where(earlier, within, 0.0)
                part = jnp.dot(
                    within.astype(jnp.bfloat16), value_tile, preferred_element_type=jnp.float32
                )
                total = suffix[:, 0:1] + drops[:, 0:1]
                if diagonal:
                    mix_old = jnp.zeros((chunk, lanes), jnp.float32)
                    carry_old = mix_old
                    if inner > 0:
                        mix_old = mix_ref[span, cols]
                        carry_old = carry_ref[span, cols]
                    mix_ref[span, cols] = jnp.where(mine, part, mix_old)
                    carry_ref[span, cols] = jnp.where(mine, total, carry_old)
                else:
                    mix_old = mix_ref[span, cols]
                    carry_old = carry_ref[span, cols]
                    mix_ref[span, cols] = jnp.where(
                        mine, mix_old + jnp.exp(carry_old) * part, mix_old
                    )
                    carry_ref[span, cols] = jnp.where(mine, carry_old + total, carry_old)


def diagonal_kernel(head_size, query_ref, key_ref, value_ref, bias_ref, mix_ref, carry_ref):
    attend_block(
        query_ref,
        lambda cols: key_ref[:, cols],
        lambda cols: value_ref[:, cols],
        lambda head: bias_ref[head : head + 1, :],
        mix_ref,
        carry_ref,
        head_size,
        True,
    )


def earlier_kernel(
    head_size, query_ref, pack_ref, bias_ref, mix_in, carry_in, gain_ref, out_ref, mix_ref, carry_ref
):
    rows, width = query_ref.shape
    lanes = 128 if width % 128 == 0 else width
    mix_ref[...] = mix_in[...]
    carry_ref[...] = carry_in[...]
    own = lax.axis_index("sp")

    def visit(step, nothing):
        block = own - 1 - step
        attend_block(
            query_ref,
            lambda cols: pack_ref[block, :rows, cols],
            lambda cols: pack_ref[block, :rows, slice(width + cols.start, width + cols.stop)],
            lambda head: bias_ref[block, head : head + 1, :],
            mix_ref,
            carry_ref,
            head_size,
            False,
        )
        return nothing

    lax.fori_loop(0, own, visit, 0)
    lane_head = lax.broadcasted_iota(jnp.int32, (1, lanes), 1) // head_size
    for group in range(width // lanes):
        cols = slice(group * lanes, (group + 1) * lanes)
        mixture = mix_ref[:, cols]
        squares = mixture * mixture
        scaled = mixture
        for inner in range(lanes // head_size):
            mine = lane_head == inner
            mean = jnp.sum(jnp.where(mine, squares, 0.0), axis=1, keepdims=True) / head_size
            scaled = jnp.where(mine, mixture * lax.rsqrt(mean + epsilon), scaled)
        out_ref[:, cols] = (scaled * gain_ref[:, cols]).astype(jnp.bfloat16)


def attention(queries, keys, values, key_bias, head_gain):
    rows, width = queries.shape
    heads, head_size = head_gain.shape
    blocks = lax.axis_size("sp")
    bias_own = key_bias.T
    extra = -(-heads * rows // (2 * width))
    padded = -(-(rows + extra) // 8) * 8 - rows
    flat_bias = jnp.pad(bias_own.reshape(-1), (0, padded * 2 * width - heads * rows))
    packed = jnp.concatenate(
        [jnp.concatenate([keys, values], axis=1), flat_bias.reshape(padded, 2 * width)], axis=0
    )
    gathered = lax.all_gather(packed, "sp", axis=0)
    vmem = pl.BlockSpec(memory_space=pltpu.VMEM)
    state = jax.ShapeDtypeStruct((rows, width), jnp.float32)
    work = heads * rows * rows
    mix, carry = pl.pallas_call(
        functools.partial(diagonal_kernel, head_size),
        out_shape=[state, state],
        in_specs=[vmem] * 4,
        out_specs=[vmem] * 2,
        cost_estimate=pl.CostEstimate(flops=work * 2000, bytes_accessed=10**6, transcendentals=0),
    )(queries, keys, values, bias_own.astype(jnp.float32))
    bias_all = gathered[:, rows:].reshape(blocks, -1)[:, : heads * rows]
    bias_all = bias_all.reshape(blocks, heads, rows).astype(jnp.float32)
    return pl.pallas_call(
        functools.partial(earlier_kernel, head_size),
        out_shape=jax.ShapeDtypeStruct((rows, width), jnp.bfloat16),
        in_specs=[vmem] * 6,
        out_specs=vmem,
        scratch_shapes=[pltpu.VMEM((rows, width), jnp.float32)] * 2,
        cost_estimate=pl.CostEstimate(flops=work * 4000, bytes_accessed=10**6, transcendentals=0),
    )(queries, gathered, bias_all, mix, carry, head_gain.reshape(1, width))


class Places:
    def __init__(self):
        self.sp = lax.axis_index("sp")
        self.tp = lax.axis_index("tp")
        self.depth = lax.axis_size("tp") // 2
        self.z = self.tp // 2
        self.core = self.tp % 2
        self.col = self.sp % 2
        self.line = self.sp // 2
        self.across = self.line * 2 + 1 - self.col
        self.along = (1 - self.line) * 2 + self.col
        self.far = (1 - self.line) * 2 + 1 - self.col
        self.partner = (self.sp, self.z * 2 + 1 - self.core)
        self.x_next = (self.across, self.tp)
        self.y_next = (self.along, self.tp)

    def z_peer(self, step):
        return lax.rem(self.z + step, self.depth)

    def z_device(self, step):
        return (self.sp, self.z_peer(step) * 2 + self.core)

    def meet(self, wide):
        barrier = pltpu.get_barrier_semaphore()
        peers = [self.partner] + [self.z_device(step) for step in range(1, self.depth)]
        if wide:
            peers = peers + [self.x_next, self.y_next]
        for peer in peers:
            pl.semaphore_signal(
                barrier, inc=1, device_id=peer, device_id_type=pl.DeviceIdType.MESH
            )
        pl.semaphore_wait(barrier, len(peers))


def remote(source, target, send_sem, recv_sem, device):
    return pltpu.make_async_remote_copy(
        src_ref=source,
        dst_ref=target,
        send_sem=send_sem,
        recv_sem=recv_sem,
        device_id=device,
        device_id_type=pl.DeviceIdType.MESH,
    )


def gather_kernel(own_ref, out_ref, local_sem, send_sems, recv_sems):
    place = Places()
    depth = place.depth
    place.meet(True)
    sends = []

    def slot(seq, z, core):
        return out_ref.at[seq, z, core]

    def send(source, seq, z, device, count):
        copy = remote(
            source,
            slot(seq, z, place.core),
            send_sems.at[count],
            recv_sems.at[seq, z, place.core],
            device,
        )
        copy.start()
        sends.append(copy)

    def arrived(seq, z, core):
        remote(
            own_ref, slot(seq, z, core), send_sems.at[0], recv_sems.at[seq, z, core], place.partner
        ).wait_recv()

    local = pltpu.make_async_copy(own_ref, slot(place.sp, place.z, place.core), local_sem)
    local.start()
    order = [0, 1] + list(range(depth - 1, 1, -1))
    for step in order[1:]:
        send(own_ref, place.sp, place.z, place.z_device(step), len(sends))
    for step in order:
        z = place.z_peer(step)
        source = own_ref
        if step > 0:
            arrived(place.sp, z, place.core)
            source = slot(place.sp, z, place.core)
        send(source, place.sp, z, place.x_next, len(sends))
        send(source, place.sp, z, place.y_next, len(sends))
        send(source, place.sp, z, place.partner, len(sends))
    for index, step in enumerate(order):
        z = place.z_peer(step)
        arrived(place.across, z, place.core)
        source = slot(place.across, z, place.core)
        if index % 2 == 0:
            send(source, place.across, z, place.y_next, len(sends))
        send(source, place.across, z, place.partner, len(sends))
        arrived(place.along, z, place.core)
        source = slot(place.along, z, place.core)
        if index % 2 == 1:
            send(source, place.along, z, place.x_next, len(sends))
        send(source, place.along, z, place.partner, len(sends))
    for step in order:
        z = place.z_peer(step)
        arrived(place.far, z, place.core)
        send(slot(place.far, z, place.core), place.far, z, place.partner, len(sends))
    for seq in (place.sp, place.across, place.along, place.far):
        for step in order:
            arrived(seq, place.z_peer(step), 1 - place.core)
    local.wait()
    for copy in sends:
        copy.wait_send()


def gather_rows(rows_in):
    rows, width = rows_in.shape
    depth = lax.axis_size("tp") // 2
    vmem = pl.BlockSpec(memory_space=pltpu.VMEM)
    count = depth - 1 + 3 * depth + 3 * depth + depth
    out = pl.pallas_call(
        gather_kernel,
        out_shape=jax.ShapeDtypeStruct((4, depth, 2, rows, width), rows_in.dtype),
        in_specs=[vmem],
        out_specs=vmem,
        scratch_shapes=[
            pltpu.SemaphoreType.DMA,
            pltpu.SemaphoreType.DMA((count,)),
            pltpu.SemaphoreType.DMA((4, depth, 2)),
        ],
        compiler_params=pltpu.CompilerParams(collective_id=1, has_side_effects=True),
    )(rows_in)
    return out.reshape(4 * depth * 2 * rows, width)


def add_into(target, first, *others):
    def one(z, nothing):
        total = first[z].astype(jnp.float32)
        for other in others:
            total = total + other[z].astype(jnp.float32)
        target[z] = total.astype(target.dtype)
        return nothing

    lax.fori_loop(0, target.shape[0], one, 0)


def finish_over_z(place, mine, z_recv, send_sems, recv_sems, base_ref, out_ref):
    copies = []
    order = [1] + list(range(place.depth - 1, 1, -1))
    for step in order:
        copy = remote(
            mine.at[place.z_peer(step)],
            z_recv.at[step - 1],
            send_sems.at[step - 1],
            recv_sems.at[step - 1],
            place.z_device(step),
        )
        copy.start()
        copies.append(copy)
    total = mine[place.z].astype(jnp.float32)
    for step, copy in zip(order, copies):
        copy.wait_recv()
        total = total + z_recv[step - 1].astype(jnp.float32)
    out_ref[...] = (base_ref[...].astype(jnp.float32) + total).astype(out_ref.dtype)
    for copy in copies:
        copy.wait_send()


def narrow_kernel(
    parts_ref, base_ref, out_ref, pair_recv, mine, z_recv, pair_send, pair_got, z_send, z_got
):
    place = Places()
    place.meet(False)
    copy = remote(
        parts_ref.at[1 - place.core], pair_recv, pair_send.at[0], pair_got.at[0], place.partner
    )
    copy.start()
    copy.wait_recv()
    add_into(mine, parts_ref.at[place.core], pair_recv)
    finish_over_z(place, mine, z_recv, z_send, z_got, base_ref, out_ref)
    copy.wait_send()


def wide_kernel(
    parts_ref,
    base_ref,
    out_ref,
    pair_recv,
    half_sum,
    x_recv,
    y_recv,
    x_last,
    y_last,
    mine,
    z_recv,
    pair_send,
    pair_got,
    xy_send,
    xy_got,
    z_send,
    z_got,
):
    place = Places()
    half = place.depth // 2
    front, back = pl.ds(0, half), pl.ds(half, place.depth - half)
    place.meet(True)
    order = (place.far, place.across, place.along, place.sp)
    pairs = []
    for count, seq in enumerate(order):
        copy = remote(
            parts_ref.at[1 - place.core, seq],
            pair_recv.at[count],
            pair_send.at[count],
            pair_got.at[count],
            place.partner,
        )
        copy.start()
        pairs.append(copy)
    sends = []

    def send(source, target, count, device):
        copy = remote(source, target, xy_send.at[count], xy_got.at[count], device)
        copy.start()
        sends.append(copy)
        return copy

    def pair_sum(count):
        pairs[count].wait_recv()
        add_into(half_sum.at[count], parts_ref.at[place.core, order[count]], pair_recv.at[count])

    pair_sum(0)
    far_x = send(half_sum.at[0, front], x_recv.at[1], 0, place.x_next)
    far_y = send(half_sum.at[0, back], y_recv.at[1], 1, place.y_next)
    pair_sum(1)
    near_x = send(half_sum.at[1, front], x_recv.at[0], 2, place.x_next)
    pair_sum(2)
    near_y = send(half_sum.at[2, back], y_recv.at[0], 3, place.y_next)
    pair_sum(3)
    far_x.wait_recv()
    add_into(x_recv.at[1], half_sum.at[2, front], x_recv.at[1])
    last_y = send(x_recv.at[1], y_last, 4, place.y_next)
    far_y.wait_recv()
    add_into(y_recv.at[1], half_sum.at[1, back], y_recv.at[1])
    last_x = send(y_recv.at[1], x_last, 5, place.x_next)
    near_x.wait_recv()
    near_y.wait_recv()
    last_y.wait_recv()
    add_into(mine.at[front], half_sum.at[3, front], x_recv.at[0], y_last)
    last_x.wait_recv()
    add_into(mine.at[back], half_sum.at[3, back], y_recv.at[0], x_last)
    finish_over_z(place, mine, z_recv, z_send, z_got, base_ref, out_ref)
    for copy in pairs + sends:
        copy.wait_send()


def scatter_sum(parts, base, out_dtype):
    rows, width = base.shape
    depth = lax.axis_size("tp") // 2
    vmem = pl.BlockSpec(memory_space=pltpu.VMEM)
    wide = parts.shape[0] > depth * 2 * rows
    half = depth // 2

    def room(*lead):
        return pltpu.VMEM(lead + (rows, width), jnp.bfloat16)

    def sems(count):
        return pltpu.SemaphoreType.DMA((count,))

    ends = [room(depth), room(depth - 1)]
    tail = [sems(depth - 1), sems(depth - 1)]
    if wide:
        shaped = parts.reshape(4, depth, 2, rows, width).transpose(2, 0, 1, 3, 4)
        body = wide_kernel
        scratch = [room(4, depth), room(4, depth), room(2, half), room(2, depth - half)]
        scratch = scratch + [room(depth - half), room(half)] + ends
        scratch = scratch + [sems(4), sems(4), sems(6), sems(6)] + tail
    else:
        shaped = parts.reshape(depth, 2, rows, width).transpose(1, 0, 2, 3)
        body = narrow_kernel
        scratch = [room(depth)] + ends + [sems(1), sems(1)] + tail
    return pl.pallas_call(
        body,
        out_shape=jax.ShapeDtypeStruct((rows, width), out_dtype),
        in_specs=[vmem] * 2,
        out_specs=vmem,
        scratch_shapes=scratch,
        compiler_params=pltpu.CompilerParams(
            collective_id=2 if wide else 0, has_side_effects=True, vmem_limit_bytes=60 * 2**20
        ),
    )(shaped, base)


def on_device(
    queries,
    keys,
    values,
    key_bias,
    head_gain,
    out_weight,
    residual,
    norm_gain,
    gate_proj,
    up_proj,
    down_proj,
    expert_choice,
    expert_weights,
):
    rows_own = queries.shape[0]
    model_width = out_weight.shape[1]
    seq_devices = lax.axis_size("sp")
    head_devices = lax.axis_size("tp")
    row_share = rows_own // head_devices
    local_experts = gate_proj.shape[0]
    experts_all = local_experts * seq_devices
    capacity = 4 * rows_own // (head_devices * experts_all)
    dense = capacity >= row_share and seq_devices == 4 and head_devices % 4 == 0
    if dense:
        named = expert_choice[:, :, None] == jnp.arange(experts_all, dtype=jnp.int32)
        own_weights = jnp.sum(jnp.where(named, expert_weights[:, :, None], 0.0), axis=1)
        all_weights = lax.all_gather(own_weights, ("sp", "tp"), axis=0, tiled=True)
        queries, all_weights = lax.optimization_barrier((queries, all_weights))
    attended = attention(queries, keys, values, key_bias, head_gain)
    shares = jnp.dot(attended, out_weight, preferred_element_type=jnp.float32)
    stream = scatter_sum(shares.astype(jnp.bfloat16), residual, jnp.bfloat16)
    normed = (rms_scaled(stream.astype(jnp.float32)) * norm_gain).astype(jnp.bfloat16)
    if dense:
        all_rows = gather_rows(normed)
        total = 0.0
        for local in range(local_experts):
            expert = lax.axis_index("sp") * local_experts + local
            weight = lax.dynamic_slice_in_dim(all_weights, expert, 1, 1)
            share = expert_partial(all_rows, gate_proj[local], up_proj[local], down_proj[local])
            total = total + jnp.where(weight > 0.0, weight * share, 0.0)
        return scatter_sum(total.astype(jnp.bfloat16), stream, jnp.bfloat16)
    own_slots = expert_choice * capacity + choice_ranks(expert_choice, experts_all)
    wanted = slot_tokens(own_slots, experts_all * capacity, row_share)
    outgoing = jnp.take(normed, wanted, axis=0, mode="fill", fill_value=0)
    arrived = lax.all_to_all(
        outgoing.reshape(seq_devices, local_experts, capacity, model_width),
        "sp",
        split_axis=0,
        concat_axis=0,
        tiled=True,
    )
    row_piece = lax.all_gather(arrived, "tp", axis=0, tiled=True)
    count_rows = row_piece.shape[0]
    partials = jnp.stack(
        [
            expert_partial(
                row_piece[:, 0].reshape(-1, model_width), gate_proj[0], up_proj[0], down_proj[0]
            ).reshape(count_rows, capacity, model_width)
        ],
        axis=1,
    )
    summed = lax.psum_scatter(partials.astype(jnp.bfloat16), "tp", scatter_dimension=0, tiled=True)
    returned = lax.all_to_all(summed, "sp", split_axis=0, concat_axis=0, tiled=True).reshape(
        experts_all * capacity, model_width
    )
    picked = jnp.take(returned, own_slots, axis=0).astype(jnp.float32)
    combined = jnp.sum(expert_weights[:, :, None] * picked, axis=1)
    return (stream.astype(jnp.float32) + combined).astype(jnp.bfloat16)


def solution(mesh):
    placed = (
        P("sp", "tp"),
        P("sp", "tp"),
        P("sp", "tp"),
        P("sp", "tp"),
        P("tp", None),
        P("tp", None),
        P(("sp", "tp"), None),
        P(),
        P("sp", None, "tp"),
        P("sp", None, "tp"),
        P("sp", "tp", None),
        P(("sp", "tp"), None),
        P(("sp", "tp"), None),
    )
    return jax.shard_map(
        on_device, mesh=mesh, in_specs=placed, out_specs=P(("sp", "tp"), None), check_vma=False
    )
```

time: 382 us -> 254 us (0.66)
  waiting for transfers between devices: 148 us -> 0.02 us
  Pallas kernels: 0 us -> 143 us
  blocking collectives: 133 us -> 43.7 us
  other arithmetic: 26.7 us -> 6.65 us
  starting transfers between devices: 8.62 us -> 0.01 us
    pallas_call x0 -> x5, Pallas kernels: none -> 143 us  [the longest x2 82.7 us: scatter_sum(): pl.pallas_call(body, out_shape=jax.ShapeDtypeStruct((rows, width), out_dt...]
    all_to_all x1 -> x0, blocking collectives: 96.4 us -> none  [on_device(): lax.all_to_all(outgoing.reshape(seq_devices, local_experts, capacity, mod...]
    reduce_scatter x1 -> x0, waiting for transfers between devices: 68.5 us -> none  [on_device(): lax.psum_scatter(partials.astype(jnp.bfloat16), 'tp', scatter_dimension=0...]
    all_gather x2 -> x1, waiting for transfers between devices: 63.6 us -> 0.01 us  [attention(): gathered = lax.all_gather(packed, 'sp', axis=0)]
    another operation x5 -> x0, other arithmetic: 15.5 us -> none
    all_to_all x2 -> x0, waiting for transfers between devices: 15.4 us -> none  [the longest x1 8.58 us: on_device(): lax.all_to_all(summed, 'sp', split_axis=0, concat_axis=0, tiled=True)]
    dot_general x4 -> x1, matrix products: 16.8 us -> 1.52 us  [on_device(): shares = jnp.dot(attended, out_weight, preferred_element_type=jnp.float32)]
    dot_general x1, matrix products: 8.73 us -> 20.3 us  [expert_partial(): return jnp.dot(hidden, down_matrix, preferred_element_type=jnp.float32)]
  transfers between devices with their start and end apart: 5 -> 1, of which waited for: 4 -> 0; matrix products, arithmetic and copies ran while one was open for 10% -> 1% of each run, Pallas kernels for 0% -> 3%
where the time goes in v1:
time: 254 us; the launch traced here: 253 us
  Pallas kernels  143 us (56%)
  blocking collectives  43.7 us (17%)
  matrix products  33.2 us (13%)
  between operations  13.5 us (5%)
  local copies, waits for them, and re-layouts  13.2 us (5%)
  other arithmetic  6.65 us (3%)
    pallas_call x2, Pallas kernels, scatter_sum(): pl.pallas_call(body, out_shape=jax.ShapeDtypeStruct((rows, width), out_dt...  82.7 us
    pallas_call x1, Pallas kernels, gather_rows(): pl.pallas_call(gather_kernel, out_shape=jax.ShapeDtypeStruct((4, depth, 2...  50.8 us
    all_gather x1, blocking collectives, on_device(): all_weights = lax.all_gather(own_weights, ('sp', 'tp'), axis=0, tiled=True)  43.7 us
    dot_general x1, matrix products, expert_partial(): return jnp.dot(hidden, down_matrix, preferred_element_type=jnp.float32)  20.3 us
    dot_general x1, matrix products, expert_partial(): jnp.dot(row_block, gate_matrix, preferred_element_type=jnp.float32)  11.3 us
    pallas_call x1, Pallas kernels, attention(): pl.pallas_call(functools.partial(diagonal_kernel, head_size), out_shape=[...  6.91 us
    reshape x1, local copies, waits for them, and re-layouts, scatter_sum(): shaped = parts.reshape(4, depth, 2, rows, width).transpose(2, 0, 1, 3, 4)  6.56 us
  transfers between devices with their start and end apart: 1, of which 0 were waited for; matrix products, arithmetic and copies ran while one was open for 1% of the time, Pallas kernels for 3%

profile of v1, /device:TPU:0, one launch (start us, length us, event | category | flops | bytes accessed | tf_op | source)
XLA Modules:
  0.0 253.4 jit_solution(2966264476389115976)
XLA Ops:
  6.5 0.0 copy-start
  6.5 0.0 all-gather.4.cloned.1.call-start
  6.5 0.8 reshape.35
  7.4 1.8 pad_maximum_fusion
  9.2 0.0 all-gather.4.cloned.1.call-update
  9.2 1.4 reshape.38.gain_ref
  10.6 0.7 select_reduce_fusion
  11.3 43.7 %all-gather.1 = f32[32,48,4]{1,2,0:T(4,128)S(1)} all-gather(f32[1,48,4]{1,2,0:T(4,128)S(1)} %bitcast.41), channel_id=1, replica_groups=mesh['sp'=4,'tp'=8] {'sp','tp'}, dimensions={0}, use_global_device_ids=true | all-gather | bytes 25344 | tf_op jit(solution)/shard_map/all_gather | solution.py:498
  55.0 0.1 reshape.45
  55.2 1.3 bitcast_convert_fusion.bias_ref
  56.4 6.9 %shard_map.127 = (f32[384,256]{1,0:T(8,128)}, f32[384,256]{1,0:T(8,128)}) custom-call(bf16[384,256]{1,0:T(8,128)(2,1)} %query_ref.1, bf16[384,256]{1,0:T(8,128)(2,1)} %key_ref.1, bf16[384,256]{1,0:T(8,128)(2,1)} %value_ref.1, f32[4,384]{1,0:T(4,128)} %bitcast_convert_fusion.bias_ref), custom_call_target="tpu_custom_call" | custom-call | flops 1179648000 | bytes 1000000 | tf_op jit(solution)/shard_map/pallas_call | solution.py:167
  63.4 0.0 all-gather.4.cloned.1.call-done
  63.4 0.8 slice_bitcast_fusion
  64.2 0.6 reshape.42.bias_ref
  64.8 2.9 %shard_map.128 = bf16[384,256]{1,0:T(8,128)(2,1)} custom-call(bf16[384,256]{1,0:T(8,128)(2,1)} %query_ref.1, bf16[4,392,512]{2,1,0:T(8,128)(2,1)} %bitcast.43, f32[4,4,384]{2,1,0:T(4,128)} %reshape.42.bias_ref, f32[384,256]{1,0:T(8,128)} %get-tuple-element.11.mix_in, f32[384,256]{1,0:T(8,128)} %get-tuple-element.12.carry_in, f32[1,256]{1,0:T(1,128)} %reshape.38.gain_ref), custom_call_target="tpu_custom_call" | custom-call | flops 2359296000 | bytes 1000000 | tf_op jit(solution)/shard_map/pallas_call | solution.py:176
  67.6 0.0 copy-done
  67.6 0.0 copy-start.1
  67.6 1.5 convolution_convert_fusion
  69.2 1.3 copy.36
  70.4 25.3 %shard_map.129.base_ref = bf16[48,2048]{1,0:T(8,128)(2,1)} custom-call(bf16[2,4,48,2048]{3,2,1,0:T(8,128)(2,1)} %bitcast.38, bf16[48,2048]{1,0:T(8,128)(2,1)} %base_ref.1), custom_call_target="tpu_custom_call" | custom-call | tf_op jit(solution)/shard_map/pallas_call | solution.py:459
  95.8 1.1 fusion.7
  96.9 0.0 copy-done.1
  96.9 1.7 fusion.9.own_ref
  98.6 50.8 %shard_map.130 = bf16[4,4,2,48,2048]{4,3,2,1,0:T(8,128)(2,1)} custom-call(bf16[48,2048]{1,0:T(8,128)(2,1)} %fusion.9.own_ref), custom_call_target="tpu_custom_call" | custom-call | tf_op jit(solution)/shard_map/pallas_call | solution.py:299
  149.4 11.3 %fusion.4 = f32[1536,896]{1,0:T(8,128)} fusion(bf16[1536,2048]{1,0:T(8,128)(2,1)} %bitcast.34, bf16[1,2048,896]{2,1,0:T(8,128)(2,1)} %param.21), kind=kOutput, calls=%fused_computation.5 | convolution fusion | flops 5637144576 | bytes 15466496 | tf_op jit(solution)/shard_map/dot_general | solution.py:18
  160.8 20.3 %select_convert_fusion = bf16[1536,2048]{1,0:T(8,128)(2,1)} fusion(f32[1536]{0:T(1024)S(1)} %dynamic-slice_reduce_fusion, pred[1536]{0:T(1024)(128)(4,1)S(1)} %compare_reduce_fusion, bf16[1,896,2048]{2,1,0:T(8,128)(2,1)} %param.23, f32[1536,896]{1,0:T(8,128)} %fusion.4, bf16[1536,2048]{1,0:T(8,128)(2,1)} %bitcast.35, bf16[1,2048,896]{2,1,0:T(8,128)(2,1)} %param.22), kind=kOutput, calls=%fused_computation | convolution fusion | flops 11291983872 | bytes 25435648 | tf_op jit(solution)/shard_map/dot_general | solution.py:21
  181.1 6.6 %copy.35 = bf16[4,4,2,48,2048]{4,3,1,0,2:T(8,128)(2,1)} copy(bf16[4,4,2,48,2048]{4,3,2,1,0:T(8,128)(2,1)} %bitcast.36) | data formatting | bytes 12582912 | tf_op jit(solution)/shard_map/reshape | solution.py:450
  187.6 57.3 %shard_map.131 = bf16[48,2048]{1,0:T(8,128)(2,1)} custom-call(bf16[2,4,4,48,2048]{4,3,2,1,0:T(8,128)(2,1)} %bitcast.33, bf16[48,2048]{1,0:T(8,128)(2,1)} %shard_map.129.base_ref), custom_call_target="tpu_custom_call" | custom-call | tf_op jit(solution)/shard_map/pallas_call | solution.py:459
  245.0 1.6 copy.38
  (8 shorter events, 0.1 us)
Async XLA Ops:
  6.5 61.1 %copy-start = (bf16[256,2048]{1,0:T(8,128)(2,1)S(1)}, bf16[256,2048]{1,0:T(8,128)(2,1)}, u32[]{:S(2)}) copy-start(bf16[256,2048]{1,0:T(8,128)(2,1)} %param.18) | copy-start | bytes 3145732
  6.5 56.8 %all-gather.4.cloned.1.call-start = ((), (), s32[]{:S(2)}) async-start(), calls=%async_computation | async-start | bytes 2007040 | tf_op jit(solution)/shard_map/all_gather | solution.py:163
  67.6 29.2 %copy-start.1 = (f32[2048]{0:T(1024)S(1)}, f32[2048]{0:T(1024)}, u32[]{:S(2)}) copy-start(f32[2048]{0:T(1024)} %param.20) | copy-start | bytes 24580
Sparse Core Ops, SparseCore 0:
  9.3 33.9 all-gather.3
